TPU v7x, 32 devices: a whole 2x2x4 slice. The times are simulated.
32 devices in a mesh: grp: 2 (over y), fs: 4 (over z), tp: 4 (over x, core).
Axes of the slice: x: 2, y: 2, z: 4, core: 2. Of those that a mesh axis runs over, the one named last changes fastest.
Arguments:
- tokens: bfloat16 [6144, 2048], P(('grp', 'fs')), parts along dimension 0, may hold values from -6 to 6
- pre_gain: float32 [2048], replicated, may hold values from 0.1 to 1.9
- up_weight: bfloat16 [2048, 8192], P('fs', 'tp'), may hold values from -0.125 to 0.125
- down_weight: bfloat16 [8192, 2048], P(('tp', 'fs')), as said below
- post_gain: float32 [2048], P('tp'), may hold values from 0.1 to 1.9
Outputs:
- mixed: bfloat16 [6144, 2048], P(('grp', 'fs'), 'tp'), parts along dimension 0
There are 2 independent parts, one for each index of `grp`. A program takes and returns all parts, laid end to end along the dimension named above; an argument that names none is the same for every part. Nothing has to cross between parts.
Inputs may be any that keep to these rules, and one draw needn't show every extreme that they name: `down_weight`: a matrix whose columns fall into 4 consecutive blocks of different magnitudes.
All inputs are finite; a program needn't handle non-finite values.
Results may differ from a plain program's by a relative error of at most 0.014.
Values may be sent and summed in bfloat16 or wider, within the bound.
A program may use at most 64 MiB of HBM per device.

v0:
```python
import jax
import jax.numpy as jnp
from jax import lax
from jax.sharding import PartitionSpec as P


def shards(tokens, pre_gain, up_weight, down_weight, post_gain):
    eps = 1e-06
    values = tokens.astype(jnp.float32)
    normed = (
        values * lax.rsqrt(jnp.mean(values * values, axis=1, keepdims=True) + eps) * pre_gain
    ).astype(jnp.bfloat16)
    full_up = lax.all_gather(up_weight, "fs", axis=0, tiled=True)
    up = jnp.dot(normed, full_up, preferred_element_type=jnp.float32)
    hidden = jnp.square(jnp.maximum(up, 0.0)).astype(jnp.bfloat16)
    full_down = lax.all_gather(down_weight, "fs", axis=0, tiled=True)
    partial_terms = jnp.dot(hidden, full_down, preferred_element_type=jnp.float32)
    own_width = post_gain.shape[0]
    full_width = lax.axis_size("tp") * own_width
    mixed = lax.psum_scatter(
        partial_terms.astype(jnp.bfloat16), "tp", scatter_dimension=1, tiled=True
    ).astype(jnp.float32)
    squares = lax.psum(jnp.sum(mixed * mixed, axis=1), "tp")
    factor = lax.rsqrt(squares / full_width + eps)
    return (mixed * factor[:, None] * post_gain).astype(jnp.bfloat16)


def solution(mesh):
    in_specs = (P(("grp", "fs"), None), P(), P("fs", "tp"), P(("tp", "fs"), None), P("tp"))
    out_specs = P(("grp", "fs"), "tp")
    return jax.shard_map(shards, mesh=mesh, in_specs=in_specs, out_specs=out_specs, check_vma=False)
```

profile of v0, /device:TPU:0, one launch (start us, length us, event | category | flops | bytes accessed | tf_op | source)
XLA Modules:
  0.0 383.3 jit_solution(18431239371068029638)
XLA Ops:
  6.5 0.0 copy-start
  6.5 0.0 copy-start.2
  6.5 0.0 all-gather.3.cloned.1.call-start
  6.5 0.7 all-gather.3.cloned.1.call-update
  7.3 0.0 all-gather.5.cloned.1.call-start
  7.3 0.7 all-gather.5.cloned.1.call-update
  8.0 0.0 reduce-scatter.2.cloned.1.call-start
  8.1 0.4 copy-done
  8.4 0.7 fusion
  9.1 0.0 copy-start.1
  9.1 152.1 %all-gather.3.cloned.1.call-done = bf16[2048,2048]{1,0:T(8,128)(2,1)} async-done(((bf16[512,2048]{1,0:T(8,128)(2,1)}), bf16[2048,2048]{1,0:T(8,128)(2,1)}) %all-gather.3.cloned.1.call-update) | async-done | bytes 8388624 | tf_op jit(solution)/shard_map/all_gather | solution.py:13
  161.3 149.4 %all-gather.5.cloned.1.call-done = bf16[2048,2048]{1,0:T(8,128)(2,1)} async-done(((bf16[512,2048]{1,0:T(8,128)(2,1)}), bf16[2048,2048]{1,0:T(8,128)(2,1)}) %all-gather.5.cloned.1.call-update) | async-done | bytes 8388624 | tf_op jit(solution)/shard_map/all_gather | solution.py:16
  310.7 0.0 copy-done.2
  310.7 20.6 %convolution_convert_fusion = bf16[768,2048]{1,0:T(8,128)(2,1)} fusion(bf16[2048,2048]{1,0:T(8,128)(2,1)} %all-gather.5.cloned.1.call-done, bf16[2048,2048]{1,0:T(8,128)(2,1)} %all-gather.3.cloned.1.call-done, bf16[768,2048]{1,0:T(8,128)(2,1)S(1)} %copy-done, f32[2048]{0:T(1024)S(1)} %copy-done.2, f32[768]{0:T(1024)S(1)} %add_rsqrt_fusion.1), kind=kOutput, calls=%fused_computation.6 | convolution fusion | flops 12897484800 | bytes 23079936 | tf_op jit(solution)/shard_map/dot_general | solution.py:17
  331.3 0.0 reduce-scatter.2.cloned.1.call-update
  331.3 36.1 %reduce-scatter.2.cloned.1.call-done = bf16[768,512]{1,0:T(8,128)(2,1)} async-done(((bf16[768,2048]{1,0:T(8,128)(2,1)}), bf16[768,512]{1,0:T(8,128)(2,1)}) %reduce-scatter.2.cloned.1.call-update) | async-done | bytes 786448 | tf_op jit(solution)/shard_map/reduce_scatter | solution.py:20
  367.4 1.4 fusion.6
  368.7 5.8 %psum.7 = f32[768]{0:T(1024)S(1)} all-reduce(f32[768]{0:T(1024)S(1)} %fusion.6), channel_id=1, replica_groups=mesh['grp'=2,'fs'=4,'tp'=4] {'tp'}, use_global_device_ids=true, to_apply=%region_3.0 | all-reduce | flops 768 | bytes 6144 | tf_op jit(solution)/shard_map/psum | solution.py:23
  374.5 0.0 copy-done.1
  374.5 2.3 fusion.8
  (2 shorter events, 0.0 us)
Async XLA Ops:
  6.5 1.9 copy-start
  6.5 304.1 %copy-start.2 = (f32[2048]{0:T(1024)S(1)}, f32[2048]{0:T(1024)}, u32[]{:S(2)}) copy-start(f32[2048]{0:T(1024)} %param.6) | copy-start | bytes 24580
  6.5 154.7 %all-gather.3.cloned.1.call-start = ((), (), s32[]{:S(2)}) async-start(), calls=%async_computation.1 | async-start | bytes 10485760 | tf_op jit(solution)/shard_map/all_gather | solution.py:13
  7.3 303.4 %all-gather.5.cloned.1.call-start = ((), (), s32[]{:S(2)}) async-start(), calls=%async_computation.2 | async-start | bytes 10485760 | tf_op jit(solution)/shard_map/all_gather | solution.py:16
  8.0 359.3 %reduce-scatter.2.cloned.1.call-start = ((), (), s32[]{:S(2)}) async-start(), calls=%async_computation.3 | async-start | bytes 3932160 | tf_op jit(solution)/shard_map/reduce_scatter | solution.py:20
  9.1 365.4 %copy-start.1 = (f32[512]{0:T(512)S(1)}, f32[512]{0:T(512)}, u32[]{:S(2)}) copy-start(f32[512]{0:T(512)} %param.9) | copy-start | bytes 6148
Sparse Core Ops, SparseCore 0:
  8.9 152.3 all-gather.2
  162.8 147.7 all-gather.4
  331.4 35.8 reduce-scatter.1
where the time goes:
time: 383 us
  waiting for transfers between devices  339 us (89%)
  matrix products  20.6 us (5%)
  between operations  13.1 us (3%)
  blocking collectives  5.77 us (2%)
  other arithmetic  4.31 us (1%)
    all_gather x1, waiting for transfers between devices, shards(): full_up = lax.all_gather(up_weight, 'fs', axis=0, tiled=True)  152 us
    all_gather x1, waiting for transfers between devices, shards(): full_down = lax.all_gather(down_weight, 'fs', axis=0, tiled=True)  149 us
    reduce_scatter x1, waiting for transfers between devices, shards(): lax.psum_scatter(partial_terms.astype(jnp.bfloat16), 'tp', scatter_dimens...  36.1 us
    dot_general x1, matrix products, shards(): jnp.dot(hidden, full_down, preferred_element_type=jnp.float32)  20.6 us
  transfers between devices with their start and end apart: 3, of which 3 were waited for; matrix products, arithmetic and copies ran while one was open for 0% of the time, Pallas kernels for 0%

commit v1 on v0

--- a/solution.py
+++ b/solution.py
@@ -10,7 +10,12 @@
     normed = (
         values * lax.rsqrt(jnp.mean(values * values, axis=1, keepdims=True) + eps) * pre_gain
     ).astype(jnp.bfloat16)
-    full_up = lax.all_gather(up_weight, "fs", axis=0, tiled=True)
+    ring = [up_weight]
+    for hop in range(3):
+        ring.append(lax.ppermute(ring[-1], "fs", [(dev, (dev + 1) % 4) for dev in range(4)]))
+    full_up = jnp.roll(
+        jnp.concatenate(ring[::-1], axis=0), (lax.axis_index("fs") + 1) * ring[0].shape[0], axis=0
+    )
     up = jnp.dot(normed, full_up, preferred_element_type=jnp.float32)
     hidden = jnp.square(jnp.maximum(up, 0.0)).astype(jnp.bfloat16)
     full_down = lax.all_gather(down_weight, "fs", axis=0, tiled=True)

time: 383 us -> 364 us (0.950)
  waiting for transfers between devices: 339 us -> 259 us
  starting transfers between devices: 0.08 us -> 54.2 us
  local copies, waits for them, and re-layouts: 0.38 us -> 8.07 us
    ppermute x0 -> x3, waiting for transfers between devices: none -> 221 us  [shards(): lax.ppermute(ring[-1], 'fs', [(dev, (dev + 1) % 4) for dev in range(4)])]
    all_gather x1 -> x0, waiting for transfers between devices: 152 us -> none  [shards(): full_up = lax.all_gather(up_weight, 'fs', axis=0, tiled=True)]
    all_gather x1, waiting for transfers between devices: 149 us -> 0.02 us  [shards(): full_down = lax.all_gather(down_weight, 'fs', axis=0, tiled=True)]
    ppermute x0 -> x3, starting transfers between devices: none -> 54.2 us  [shards(): lax.ppermute(ring[-1], 'fs', [(dev, (dev + 1) % 4) for dev in range(4)])]
    dot_general x1, matrix products: 20.6 us -> 10.3 us  [shards(): jnp.dot(hidden, full_down, preferred_element_type=jnp.float32)]
    unnamed x6 -> x15, local copies, waits for them, and re-layouts: 0.38 us -> 7.83 us
    dot_general x0 -> x1, matrix products: none -> 7.05 us  [shards(): up = jnp.dot(normed, full_up, preferred_element_type=jnp.float32)]
  transfers between devices with their start and end apart: 3 -> 5, of which waited for: 3 -> 4; matrix products, arithmetic and copies ran while one was open for 0% -> 5% of each run, Pallas kernels for 0% -> 0%
where the time goes in v1:
time: 364 us
  waiting for transfers between devices  259 us (71%)
  starting transfers between devices  54.2 us (15%)
  matrix products  17.4 us (5%)
  between operations  13.5 us (4%)
  local copies, waits for them, and re-layouts  8.07 us (2%)
  other arithmetic  6.2 us (2%)
  blocking collectives  5.77 us (2%)
    ppermute x3, waiting for transfers between devices, shards(): lax.ppermute(ring[-1], 'fs', [(dev, (dev + 1) % 4) for dev in range(4)])  221 us
    ppermute x3, starting transfers between devices, shards(): lax.ppermute(ring[-1], 'fs', [(dev, (dev + 1) % 4) for dev in range(4)])  54.2 us
    reduce_scatter x1, waiting for transfers between devices, shards(): lax.psum_scatter(partial_terms.astype(jnp.bfloat16), 'tp', scatter_dimens...  37.2 us
    dot_general x1, matrix products, shards(): jnp.dot(hidden, full_down, preferred_element_type=jnp.float32)  10.3 us
    unnamed x15, local copies, waits for them, and re-layouts  7.83 us
  transfers between devices with their start and end apart: 5, of which 4 were waited for; matrix products, arithmetic and copies ran while one was open for 5% of the time, Pallas kernels for 0%

profile of v1, /device:TPU:0, one launch (start us, length us, event | category | flops | bytes accessed | tf_op | source)
XLA Modules:
  0.0 363.7 jit_solution(4662282292436579426)
XLA Ops:
  6.5 0.0 all-gather.2.cloned.1.call-start
  6.5 0.7 all-gather.2.cloned.1.call-update
  7.3 0.0 reduce-scatter.2.cloned.1.call-start
  7.3 3.1 collective-permute-start
  10.4 81.4 %collective-permute-done = bf16[512,2048]{1,0:T(8,128)(2,1)S(1)} collective-permute-done((bf16[512,2048]{1,0:T(8,128)(2,1)}, bf16[512,2048]{1,0:T(8,128)(2,1)S(1)}, u32[]{:S(2)}, u32[]{:S(2)}) %collective-permute-start) | collective-permute-done | bytes 2097184 | tf_op jit(solution)/shard_map/ppermute | solution.py:15
  91.8 33.4 %collective-permute-start.1 = (bf16[512,2048]{1,0:T(8,128)(2,1)S(1)}, bf16[512,2048]{1,0:T(8,128)(2,1)}, u32[]{:S(2)}, u32[]{:S(2)}) collective-permute-start(bf16[512,2048]{1,0:T(8,128)(2,1)S(1)} %collective-permute-done), channel_id=1, source_target_pairs={{0,4},{4,8},{8,12},{12,0},{1,5},{5,9},{9,13},{13,1},{2,6},{6,10},{... | collective-permute-start | bytes 6291464 | tf_op jit(solution)/shard_map/ppermute | solution.py:15
  125.2 93.9 %collective-permute-done.1 = bf16[512,2048]{1,0:T(8,128)(2,1)} collective-permute-done((bf16[512,2048]{1,0:T(8,128)(2,1)S(1)}, bf16[512,2048]{1,0:T(8,128)(2,1)}, u32[]{:S(2)}, u32[]{:S(2)}) %collective-permute-start.1) | collective-permute-done | bytes 2097184 | tf_op jit(solution)/shard_map/ppermute | solution.py:15
  219.1 17.7 %collective-permute-start.2 = (bf16[512,2048]{1,0:T(8,128)(2,1)}, bf16[512,2048]{1,0:T(8,128)(2,1)}, u32[]{:S(2)}, u32[]{:S(2)}) collective-permute-start(bf16[512,2048]{1,0:T(8,128)(2,1)} %collective-permute-done.1), channel_id=1, source_target_pairs={{0,4},{4,8},{8,12},{12,0},{1,5},{5,9},{9,13},{13,1},{2,6},{6,10},{... | collective-permute-start | bytes 6291464 | tf_op jit(solution)/shard_map/ppermute | solution.py:15
  236.8 2.6 fusion.2
  239.4 0.0 copy-start
  239.4 45.2 %collective-permute-done.2 = bf16[512,2048]{1,0:T(8,128)(2,1)} collective-permute-done((bf16[512,2048]{1,0:T(8,128)(2,1)}, bf16[512,2048]{1,0:T(8,128)(2,1)}, u32[]{:S(2)}, u32[]{:S(2)}) %collective-permute-start.2) | collective-permute-done | bytes 2097184 | tf_op jit(solution)/shard_map/ppermute | solution.py:15
  284.6 1.7 constant_dynamic-update-slice_fusion.7
  286.4 1.7 constant_dynamic-update-slice_fusion.6
  288.1 0.1 constant_dynamic-update-slice_fusion.5
  288.2 0.0 copy-done
  288.2 0.2 constant_dynamic-update-slice_fusion.4
  288.5 1.7 constant_dynamic-update-slice_fusion.3
  290.2 0.0 copy-start.1
  290.2 0.0 copy-start.3
  290.2 1.9 constant_dynamic-update-slice_fusion.2
  292.1 0.1 constant_dynamic-update-slice_fusion.1
  292.3 0.2 constant_dynamic-update-slice_fusion
  292.5 0.2 copy-done.1
  292.7 0.0 copy-done.3
  292.8 7.1 %multiply_convert_fusion = bf16[768,2048]{1,0:T(8,128)(2,1)S(1)} fusion(bf16[4096,2048]{1,0:T(8,128)(2,1)S(1)} %constant_dynamic-update-slice_fusion, s32[]{:T(128)S(6)} %select_n.14, bf16[768,2048]{1,0:T(8,128)(2,1)S(1)} %copy-done.1, f32[2048]{0:T(1024)S(1)} %copy-done.3, f32[768]{0:T(1024)S(1)} %add_rsqrt_fusion.1), kind=kOutput, calls=%fused_computation.7 | convolution fusion | flops 6453460992 | bytes 14692356 | tf_op jit(solution)/shard_map/dot_general | solution.py:19
  299.8 0.0 copy-start.2
  299.8 0.0 all-gather.2.cloned.1.call-done
  299.9 10.3 %convolution_convert_fusion = bf16[768,2048]{1,0:T(8,128)(2,1)} fusion(bf16[768,2048]{1,0:T(8,128)(2,1)S(1)} %multiply_convert_fusion, bf16[2048,2048]{1,0:T(8,128)(2,1)} %all-gather.2.cloned.1.call-done), kind=kOutput, calls=%fused_computation.8 | convolution fusion | flops 6444023808 | bytes 14680064 | tf_op jit(solution)/shard_map/dot_general | solution.py:22
  310.2 0.0 reduce-scatter.2.cloned.1.call-update
  310.2 37.2 %reduce-scatter.2.cloned.1.call-done = bf16[768,512]{1,0:T(8,128)(2,1)} async-done(((bf16[768,2048]{1,0:T(8,128)(2,1)}), bf16[768,512]{1,0:T(8,128)(2,1)}) %reduce-scatter.2.cloned.1.call-update) | async-done | bytes 786448 | tf_op jit(solution)/shard_map/reduce_scatter | solution.py:25
  347.4 1.4 fusion.10
  348.8 5.8 %psum.7 = f32[768]{0:T(1024)S(1)} all-reduce(f32[768]{0:T(1024)S(1)} %fusion.10), channel_id=1, replica_groups=mesh['grp'=2,'fs'=4,'tp'=4] {'tp'}, use_global_device_ids=true, to_apply=%region_3.4 | all-reduce | flops 768 | bytes 6144 | tf_op jit(solution)/shard_map/psum | solution.py:28
  354.6 0.0 copy-done.2
  354.6 2.3 fusion.12
  (2 shorter events, 0.0 us)
Async XLA Ops:
  6.5 293.3 %all-gather.2.cloned.1.call-start = ((), (), s32[]{:S(2)}) async-start(), calls=%async_computation.1 | async-start | bytes 10485760 | tf_op jit(solution)/shard_map/all_gather | solution.py:21
  7.3 340.2 %reduce-scatter.2.cloned.1.call-start = ((), (), s32[]{:S(2)}) async-start(), calls=%async_computation.2 | async-start | bytes 3932160 | tf_op jit(solution)/shard_map/reduce_scatter | solution.py:25
  7.3 84.5 %collective-permute-start = (bf16[512,2048]{1,0:T(8,128)(2,1)}, bf16[512,2048]{1,0:T(8,128)(2,1)S(1)}, u32[]{:S(2)}, u32[]{:S(2)}) collective-permute-start(bf16[512,2048]{1,0:T(8,128)(2,1)} %param.7), channel_id=1, source_target_pairs={{0,4},{4,8},{8,12},{12,0},{1,5},{5,9},{9,13},{13,1},{2,6},{6,10},{... | collective-permute-start | bytes 6291464 | tf_op jit(solution)/shard_map/ppermute | solution.py:15
  91.8 127.3 %collective-permute-start.1 = (bf16[512,2048]{1,0:T(8,128)(2,1)S(1)}, bf16[512,2048]{1,0:T(8,128)(2,1)}, u32[]{:S(2)}, u32[]{:S(2)}) collective-permute-start(bf16[512,2048]{1,0:T(8,128)(2,1)S(1)} %collective-permute-done), channel_id=1, source_target_pairs={{0,4},{4,8},{8,12},{12,0},{1,5},{5,9},{9,13},{13,1},{2,6},{6,10},{... | collective-permute-start | bytes 6291464 | tf_op jit(solution)/shard_map/ppermute | solution.py:15
  219.1 65.5 %collective-permute-start.2 = (bf16[512,2048]{1,0:T(8,128)(2,1)}, bf16[512,2048]{1,0:T(8,128)(2,1)}, u32[]{:S(2)}, u32[]{:S(2)}) collective-permute-start(bf16[512,2048]{1,0:T(8,128)(2,1)} %collective-permute-done.1), channel_id=1, source_target_pairs={{0,4},{4,8},{8,12},{12,0},{1,5},{5,9},{9,13},{13,1},{2,6},{6,10},{... | collective-permute-start | bytes 6291464 | tf_op jit(solution)/shard_map/ppermute | solution.py:15
  239.4 48.8 %copy-start = (bf16[512,2048]{1,0:T(8,128)(2,1)S(1)}, bf16[512,2048]{1,0:T(8,128)(2,1)}, u32[]{:S(2)}) copy-start(bf16[512,2048]{1,0:T(8,128)(2,1)} %param.7) | copy-start | bytes 6291460
  290.2 2.5 copy-start.1
  290.2 2.5 copy-start.3
  299.8 54.7 %copy-start.2 = (f32[512]{0:T(512)S(1)}, f32[512]{0:T(512)}, u32[]{:S(2)}) copy-start(f32[512]{0:T(512)} %param.9) | copy-start | bytes 6148
Sparse Core Ops, SparseCore 0:
  8.9 229.6 all-gather.1
  310.3 37.0 reduce-scatter.1
